TPU v7x, 128 devices: a whole 4x4x4 slice. The times are simulated.
128 devices in a mesh: rep: 2 (over z_hi), fs: 32 (over z_lo, y, x), tp: 2 (over core).
Axes of the slice: x: 4, y: 4, z: 4 (z_hi: 2, z_lo: 2; z = z_hi * 2 + z_lo), core: 2. Of those that a mesh axis runs over, the one named last changes fastest.
Arguments:
- tokens: bfloat16 [65536, 2048], P(('rep', 'fs', 'tp')), parts along dimension 0, may hold values from -6 to 6
- mix_gain: float32 [2048], replicated, may hold values from 0.1 to 1.9
- w_query: bfloat16 [2048, 512], P('fs', 'tp'), may hold values from -0.125 to 0.125
- w_key: bfloat16 [2048, 512], P('fs', 'tp'), may hold values from -0.125 to 0.125
- w_value: bfloat16 [2048, 1024], P('fs', 'tp'), may hold values from -0.125 to 0.125
- w_out: bfloat16 [1024, 2048], P('tp', 'fs'), may hold values from -0.1875 to 0.1875
- ffn_gain: float32 [2048], replicated, may hold values from 0.1 to 1.9
- w_ffgate: bfloat16 [2048, 2816], P('fs', 'tp'), may hold values from -0.125 to 0.125
- w_ffup: bfloat16 [2048, 2816], P('fs', 'tp'), may hold values from -0.125 to 0.125
- conv_gate: float32 [3, 2816], replicated, may hold values from -3 to 3
- conv_up: float32 [3, 2816], replicated, may hold values from -3 to 3
- w_down: bfloat16 [2816, 2048], P('tp', 'fs'), may hold values from -0.109375 to 0.109375
Outputs:
- layer_out: bfloat16 [65536, 2048], P(('rep', 'fs', 'tp')), parts along dimension 0
There are 2 independent parts, one for each index of `rep`. A program takes and returns all parts, laid end to end along the dimension named above; an argument that names none is the same for every part. Nothing has to cross between parts.
All inputs are finite; a program needn't handle non-finite values.
Results may differ from a plain program's by a relative error of at most 0.014.
Values may be sent and summed in bfloat16 or wider, within the bound.
No kernel may reach another device: no remote copies, remote signals or barrier semaphores. Data moves between devices by JAX's collectives and lax.ppermute only.
A program may use at most 128 MiB of HBM per device.

v0:
```python
import jax
import jax.numpy as jnp
from jax import lax
from jax.sharding import PartitionSpec as P

HEADS = 4
DK = 128
DV = 256
KERNEL = 3
BLOCK = 128
LENGTH = 1024
epsilon = 1e-06


def in_one_piece(arrays, axis, dim, along):
    both = jnp.concatenate(arrays, axis=along)
    out, at, done = (lax.all_gather(both, axis, axis=dim, tiled=True), 0, [])
    for a in arrays:
        done.append(lax.slice_in_dim(out, at, at + a.shape[along], axis=along))
        at += a.shape[along]
    return tuple(done)


def copy_for_each(shard, axis):
    length = lax.axis_size(axis)
    return lax.all_to_all(
        jnp.broadcast_to(shard[None], (length, *shard.shape)), axis, 0, 0, tiled=True
    )


def in_order(pieces, dim):
    pieces = jnp.moveaxis(pieces, 0, dim)
    dims = pieces.shape
    return pieces.reshape(*dims[:dim], dims[dim] * dims[dim + 1], *dims[dim + 2 :])


def collect(shard, axis, dim):
    pieces = copy_for_each(shard, axis)
    return in_order(pieces, dim)


def in_blocks(shard, dim, length):
    dims = shard.shape
    pieces = shard.reshape(*dims[:dim], length, dims[dim] // length, *dims[dim + 1 :])
    return jnp.moveaxis(pieces, dim, 0)


def sent_and_summed(shard, axis, dim):
    length = lax.axis_size(axis)
    pieces = lax.all_to_all(in_blocks(shard, dim, length), axis, 0, 0, tiled=True)
    return jnp.sum(pieces.astype(jnp.float32), axis=0)


def rms_rows(matrix, scale_vec):
    values = matrix.astype(jnp.float32)
    factor = lax.rsqrt(jnp.mean(values * values, axis=-1, keepdims=True) + epsilon)
    return (values * factor * scale_vec).astype(jnp.bfloat16)


def rotate_heads(matrix):
    length = matrix.shape[0]
    half_width = matrix.shape[-1] // 2
    inverse = 10000.0 ** (-jnp.arange(half_width, dtype=jnp.float32) * 2.0 / (2 * half_width))
    angles = jnp.arange(length, dtype=jnp.float32)[:, None] * inverse[None, :]
    cosine = jnp.cos(angles)[:, None, :]
    sine = jnp.sin(angles)[:, None, :]
    values = matrix.astype(jnp.float32)
    first_half = values[..., :half_width]
    second_half = values[..., half_width:]
    return jnp.concatenate(
        [first_half * cosine - second_half * sine, first_half * sine + second_half * cosine],
        axis=-1,
    )


def retain_blocks(rot_query, rot_key, value, rates, block_len):
    length, head_count, width_k = rot_query.shape
    width_v = value.shape[-1]
    blocks = length // block_len
    query4 = rot_query.reshape(blocks, block_len, head_count, width_k)
    key4 = rot_key.reshape(blocks, block_len, head_count, width_k)
    value4 = value.reshape(blocks, block_len, head_count, width_v)
    places = jnp.arange(block_len, dtype=jnp.float32)
    spacing = places[:, None] - places[None, :]
    inside = jnp.where(
        spacing[None] >= 0, jnp.exp(-jnp.maximum(spacing, 0.0)[None] * rates[:, None, None]), 0.0
    )
    scores = jnp.einsum("cihd,cjhd->chij", query4, key4, preferred_element_type=jnp.float32)
    weights = (scores * inside[None]).astype(jnp.bfloat16)
    inner_part = jnp.einsum("chij,cjhe->cihe", weights, value4, preferred_element_type=jnp.float32)
    tail_decay = jnp.exp(-(block_len - 1.0 - places)[:, None] * rates[None, :])
    decayed = (key4.astype(jnp.float32) * tail_decay[None, :, :, None]).astype(jnp.bfloat16)
    states = jnp.einsum("cjhd,cjhe->chde", decayed, value4, preferred_element_type=jnp.float32)
    passing = jnp.exp(-block_len * rates)[:, None, None]

    def advance(carried, fresh):
        return (carried * passing + fresh, carried)

    _, before = lax.scan(advance, jnp.zeros((head_count, width_k, width_v), jnp.float32), states)
    onset_decay = jnp.exp(-(places + 1.0)[:, None] * rates[None, :])
    cross_part = (
        jnp.einsum("cihd,chde->cihe", query4.astype(jnp.float32), before)
        * onset_decay[None, :, :, None]
    )
    return (inner_part + cross_part).reshape(length, head_count, width_v)


def head_norm(retained):
    average = jnp.mean(retained, axis=-1, keepdims=True)
    centered = retained - average
    return centered * lax.rsqrt(jnp.mean(centered * centered, axis=-1, keepdims=True) + epsilon)


def causal_taps(matrix, kernel_w):
    length = matrix.shape[0]
    padded = jnp.pad(matrix.astype(jnp.float32), ((KERNEL - 1, 0), (0, 0)))
    total = jnp.zeros((length, matrix.shape[1]), jnp.float32)
    for tap_idx in range(KERNEL):
        total = total + kernel_w[tap_idx][None, :] * padded[tap_idx : tap_idx + length]
    return total


def collect_ffn(w_ffgate, w_ffup):
    return in_one_piece((w_ffgate, w_ffup), "fs", 0, 1)


def body(
    tokens,
    mix_gain,
    w_query,
    w_key,
    w_value,
    w_out,
    ffn_gain,
    w_ffgate,
    w_ffup,
    conv_gate,
    conv_up,
    w_down,
):
    tp_rank = lax.axis_index("tp")
    heads_here = w_query.shape[1] // DK
    ffn_pair = None
    normed = rms_rows(tokens, mix_gain)
    query_w, key_w, value_w = in_one_piece((w_query, w_key, w_value), "fs", 0, 1)
    qk_cols = query_w.shape[1]
    pieces = lax.all_gather(normed, "tp", axis=0, tiled=True)
    joined = jnp.concatenate(
        [
            jnp.dot(pieces, query_w, preferred_element_type=jnp.float32),
            jnp.dot(pieces, key_w, preferred_element_type=jnp.float32),
            jnp.dot(pieces, value_w, preferred_element_type=jnp.float32),
        ],
        axis=1,
    ).astype(jnp.bfloat16)
    length = joined.shape[0]
    query = joined[:, :qk_cols].reshape(length, heads_here, DK)
    key = joined[:, qk_cols : 2 * qk_cols].reshape(length, heads_here, DK)
    value = joined[:, 2 * qk_cols :].reshape(length, heads_here, DV)
    rot_query = rotate_heads(query).astype(jnp.bfloat16)
    rot_key = (rotate_heads(key) * DK ** (-0.5)).astype(jnp.bfloat16)
    head_ids = (tp_rank * heads_here + jnp.arange(heads_here, dtype=jnp.int32)).astype(jnp.float32)
    rates = 1.0 / 16.0 * (32.0 / LENGTH) ** (head_ids / (HEADS - 1))
    retained = retain_blocks(rot_query, rot_key, value, rates, BLOCK)
    hidden = head_norm(retained).reshape(length, heads_here * DV).astype(jnp.bfloat16)
    out_full = collect(w_out, "fs", 1)
    mix_sum = sent_and_summed(
        jnp.dot(hidden, out_full, preferred_element_type=jnp.float32).astype(jnp.bfloat16), "tp", 0
    )
    resid = (tokens.astype(jnp.float32) + mix_sum).astype(jnp.bfloat16)
    normed_ffn = rms_rows(resid, ffn_gain)
    ff_here = w_ffgate.shape[1]
    ffn_pair = collect_ffn(w_ffgate, w_ffup)
    gate_w, up_w = ffn_pair
    pieces = lax.all_gather(normed_ffn, "tp", axis=0, tiled=True)
    both_pre = jnp.concatenate(
        [
            jnp.dot(pieces, gate_w, preferred_element_type=jnp.float32),
            jnp.dot(pieces, up_w, preferred_element_type=jnp.float32),
        ],
        axis=1,
    ).astype(jnp.bfloat16)
    gate_pre = both_pre[:, :ff_here]
    up_pre = both_pre[:, ff_here:]
    gate_taps = lax.dynamic_slice_in_dim(conv_gate, tp_rank * ff_here, ff_here, 1)
    up_taps = lax.dynamic_slice_in_dim(conv_up, tp_rank * ff_here, ff_here, 1)
    activ = (jax.nn.silu(causal_taps(gate_pre, gate_taps)) * causal_taps(up_pre, up_taps)).astype(
        jnp.bfloat16
    )
    down_full = lax.all_gather(w_down, "fs", axis=1, tiled=True)
    ffn_sum = sent_and_summed(
        jnp.dot(activ, down_full, preferred_element_type=jnp.float32).astype(jnp.bfloat16), "tp", 0
    )
    return (resid.astype(jnp.float32) + ffn_sum).astype(jnp.bfloat16)


def solution(mesh):
    placed = (
        P(("rep", "fs", "tp"), None),
        P(),
        P("fs", "tp"),
        P("fs", "tp"),
        P("fs", "tp"),
        P("tp", "fs"),
        P(),
        P("fs", "tp"),
        P("fs", "tp"),
        P(),
        P(),
        P("tp", "fs"),
    )
    return jax.shard_map(
        body, mesh=mesh, in_specs=placed, out_specs=P(("rep", "fs", "tp"), None), check_vma=False
    )
```

profile of v0, /device:TPU:1, one launch (start us, length us, event | category | flops | bytes accessed | tf_op | source)
XLA Modules:
  0.0 637.9 jit_solution(8390424234193751009)
XLA Ops:
  6.6 2.1 fusion.6
  8.7 3.5 fusion.8
  12.3 0.7 pad_maximum_fusion.2
  13.0 1.5 broadcast_in_dim.25
  14.5 9.3 %all-to-all-start = ((bf16[32,512,64]{1,2,0:T(8,128)(2,1)}), bf16[32,512,64]{1,2,0:T(8,128)(2,1)}, u32[]{:S(2)}, u32[]{:S(2)}) async-start(bf16[32,512,64]{1,2,0:T(8,128)(2,1)} %broadcast_in_dim.25), calls=%async_computation | async-start | bytes 4194304 | tf_op jit(solution)/shard_map/all_to_all | solution.py:26
  24.2 1.0 fusion.44
  25.2 7.1 %all-gather.6.cloned.1.call-done = bf16[1024,2048]{1,0:T(8,128)(2,1)} async-done(((bf16[512,2048]{1,0:T(8,128)(2,1)}), bf16[1024,2048]{1,0:T(8,128)(2,1)}) %all-gather.6.cloned.1.call-update) | async-done | bytes 4194320 | tf_op jit(solution)/shard_map/all_gather | solution.py:147
  32.3 140.7 %all-gather.8.cloned.1.call-done = bf16[2048,1024]{1,0:T(8,128)(2,1)} async-done(((bf16[64,1024]{1,0:T(8,128)(2,1)}), bf16[2048,1024]{1,0:T(8,128)(2,1)}) %all-gather.8.cloned.1.call-update) | async-done | bytes 4194320 | tf_op jit(solution)/shard_map/all_gather | solution.py:17
  173.0 3.9 convolution_convert_fusion.3
  177.0 0.1 convert.17
  177.1 2.5 convolution_convert_fusion.2
  179.6 0.1 convert.18
  179.7 1.1 subtract_convert_fusion
  180.9 0.4 copy.40
  181.4 0.4 copy.41
  181.8 6.2 fusion.31
  187.9 1.3 reshape_reshape.3
  189.3 0.3 fusion.37
  189.6 0.8 copy-done.1
  190.4 0.6 fusion.38
  191.0 6.5 %while.13 = (s32[]{:T(128)}, f32[2,128,256]{2,1,0:T(8,128)S(1)}, bf16[8,2,128,256]{3,2,1,0:T(8,128)(2,1)}, f32[8,2,128,256]{3,2,1,0:T(8,128)S(1)}, s32[]{:T(128)}, /*index=5*/s32[]{:T(128)}, s32[]{:T(128)}) while((s32[]{:T(128)}, f32[2,128,256]{2,1,0:T(8,128)S(1)}, bf16[8,2,128,256]{3,2,1,0:T(8,128)(2,1)}, ...), condition=%wide.region_2.3_spmd.clone, body=%wide.region_1.2_spmd.clone.sunk | while | flops 262155 | bytes 1180272 | solution.py:99
  191.0 0.7 bitcast_dynamic-update-slice_fusion.2
  191.7 0.1 bitcast_add_fusion.2
  191.8 0.7 bitcast_dynamic-update-slice_fusion.2
  192.5 0.1 bitcast_add_fusion.2
  192.6 0.7 bitcast_dynamic-update-slice_fusion.2
  193.3 0.1 bitcast_add_fusion.2
  193.4 0.7 bitcast_dynamic-update-slice_fusion.2
  194.1 0.1 bitcast_add_fusion.2
  194.3 0.7 bitcast_dynamic-update-slice_fusion.2
  194.9 0.1 bitcast_add_fusion.2
  195.1 0.7 bitcast_dynamic-update-slice_fusion.2
  195.8 0.1 bitcast_add_fusion.2
  195.9 0.7 bitcast_dynamic-update-slice_fusion.2
  196.6 0.1 bitcast_add_fusion.2
  196.7 0.7 bitcast_dynamic-update-slice_fusion.2
  197.5 1.0 copy.48
  198.5 0.3 copy.38
  198.8 1.2 copy.49
  200.0 0.3 copy.39
  200.3 3.2 fusion.45
  203.6 3.0 fusion.54
  206.6 0.1 copy.45
  206.8 0.7 multiply_reduce_fusion
  207.5 0.9 fusion.29
  208.3 0.5 copy.46
  208.9 4.0 convolution_convert_fusion.1
  212.9 27.5 %all_to_all.15 = bf16[2,512,2048]{2,1,0:T(8,128)(2,1)S(1)} all-to-all(bf16[2,512,2048]{2,1,0:T(8,128)(2,1)S(1)} %bitcast.73), channel_id=1, replica_groups=mesh['rep'=2,'fs'=32,'tp'=2] {'tp'}, dimensions={0} | all-to-all | bytes 8388608 | tf_op jit(solution)/shard_map/all_to_all | solution.py:50
  240.4 1.0 convert_reduce_fusion.1
  241.3 0.6 copy-done
  241.9 0.7 fusion.10
  242.7 1.9 fusion.12
  244.6 0.8 pad_maximum_fusion.1
  245.5 0.5 all-gather.14.cloned.1.call-update
  246.0 1.1 dynamic-slice_reduce_fusion.2
  247.1 15.1 %all-gather.10.cloned.1.call-done = bf16[1024,2048]{1,0:T(8,128)(2,1)} async-done(((bf16[512,2048]{1,0:T(8,128)(2,1)}), bf16[1024,2048]{1,0:T(8,128)(2,1)}) %all-gather.10.cloned.1.call-update) | async-done | bytes 4194320 | tf_op jit(solution)/shard_map/all_gather | solution.py:175
  262.2 155.1 %all-gather.12.cloned.1.call-done = bf16[2048,2816]{1,0:T(8,128)(2,1)} async-done(((bf16[64,2816]{1,0:T(8,128)(2,1)}), bf16[2048,2816]{1,0:T(8,128)(2,1)}) %all-gather.12.cloned.1.call-update) | async-done | bytes 11534352 | tf_op jit(solution)/shard_map/all_gather | solution.py:17
  417.3 11.8 %fusion.17 = f32[1024,1408]{1,0:T(8,128)} fusion(bf16[1024,2048]{1,0:T(8,128)(2,1)} %all-gather.10.cloned.1.call-done, bf16[2048,2816]{1,0:T(8,128)(2,1)} %all-gather.12.cloned.1.call-done), kind=kOutput, calls=%fused_computation.26 | convolution fusion | flops 5908463616 | bytes 15728640 | tf_op jit(solution)/shard_map/dot_general | solution.py:178
  429.1 8.5 %fusion.23 = f32[1024,1408]{1,0:T(8,128)} fusion(bf16[1024,2048]{1,0:T(8,128)(2,1)S(1)} %copy-done.13, bf16[2048,2816]{1,0:T(8,128)(2,1)S(1)} %copy-done.11), kind=kOutput, calls=%fused_computation.28 | convolution fusion | flops 5908463616 | bytes 15728640 | tf_op jit(solution)/shard_map/dot_general | solution.py:179
  437.6 139.5 %all-gather.14.cloned.1.call-done = bf16[1408,2048]{0,1:T(8,128)(2,1)} async-done(((bf16[1408,64]{0,1:T(8,128)(2,1)}), bf16[1408,2048]{0,1:T(8,128)(2,1)}) %all-gather.14.cloned.1.call-update) | async-done | bytes 5767184 | tf_op jit(solution)/shard_map/all_gather | solution.py:190
  577.1 23.0 %convolution_convert_fusion = bf16[1024,2048]{1,0:T(8,128)(2,1)} fusion(bf16[1408,2048]{0,1:T(8,128)(2,1)} %all-gather.14.cloned.1.call-done, f32[1024,1408]{1,0:T(8,128)} %fusion.23, f32[1024,1408]{1,0:T(8,128)} %fusion.17, f32[1408]{0:T(1024)S(1)} %get-tuple-element.59, f32[1408]{0:T(1024)S(1)} %get-tuple-element.58, f32[1408]{0:T(1024)S(1)} %get-tuple-element.57, ...), kind=kOutput, calls=%fused_computation.29 | convolution fusion | flops 5930745856 | bytes 21529600 | tf_op jit(solution)/shard_map/dot_general | solution.py:192
  600.1 28.2 %all_to_all.16 = bf16[2,512,2048]{2,1,0:T(8,128)(2,1)S(1)} all-to-all(bf16[2,512,2048]{2,1,0:T(8,128)(2,1)} %bitcast.72), channel_id=1, replica_groups=mesh['rep'=2,'fs'=32,'tp'=2] {'tp'}, dimensions={0} | all-to-all | bytes 8388608 | tf_op jit(solution)/shard_map/all_to_all | solution.py:50
  628.3 1.0 convert_reduce_fusion
  629.3 2.1 fusion.13
  (60 shorter events, 1.0 us)
Async XLA Ops:
  6.5 5.7 copy-start.7
  6.5 5.7 copy-start.8
  6.5 5.7 copy-start.9
  6.5 6.4 %copy-start.6 = (bf16[512,64]{0,1:T(8,128)(2,1)S(1)}, bf16[512,64]{0,1:T(8,128)(2,1)}, u32[]{:S(2)}) copy-start(bf16[512,64]{0,1:T(8,128)(2,1)} %param.19) | copy-start | bytes 196612
  6.5 25.8 %all-gather.6.cloned.1.call-start = ((), (), s32[]{:S(2)}) async-start(), calls=%async_computation.3 | async-start | bytes 6291456 | tf_op jit(solution)/shard_map/all_gather | solution.py:147
  12.2 160.8 %all-gather.8.cloned.1.call-start = ((), (), s32[]{:S(2)}) async-start(), calls=%async_computation.4 | async-start | bytes 4325376 | tf_op jit(solution)/shard_map/all_gather | solution.py:17
  14.5 194.4 %all-to-all-start = ((bf16[32,512,64]{1,2,0:T(8,128)(2,1)}), bf16[32,512,64]{1,2,0:T(8,128)(2,1)}, u32[]{:S(2)}, u32[]{:S(2)}) async-start(bf16[32,512,64]{1,2,0:T(8,128)(2,1)} %broadcast_in_dim.25), calls=%async_computation | async-start | bytes 4194304 | tf_op jit(solution)/shard_map/all_to_all | solution.py:26
  23.9 238.3 %all-gather.10.cloned.1.call-start = ((), (), s32[]{:S(2)}) async-start(), calls=%async_computation.5 | async-start | bytes 6291456 | tf_op jit(solution)/shard_map/all_gather | solution.py:175
  173.0 4.1 copy-start.12
  189.6 0.8 copy-start.1
  198.8 4.8 copy-start.2
  200.3 3.2 copy-start.3
  240.4 1.6 copy-start
  241.9 0.7 copy-start.10
  242.6 2.0 copy-start.4
  242.6 2.0 copy-start.5
  244.6 172.7 %all-gather.12.cloned.1.call-start = ((), (), s32[]{:S(2)}) async-start(), calls=%async_computation.6 | async-start | bytes 11894784 | tf_op jit(solution)/shard_map/all_gather | solution.py:17
  245.4 331.7 %all-gather.14.cloned.1.call-start = ((), (), s32[]{:S(2)}) async-start(), calls=%async_computation.7 | async-start | bytes 5947392 | tf_op jit(solution)/shard_map/all_gather | solution.py:190
  417.3 11.8 %copy-start.11 = (bf16[2048,2816]{1,0:T(8,128)(2,1)S(1)}, bf16[2048,2816]{1,0:T(8,128)(2,1)}, u32[]{:S(2)}) copy-start(bf16[2048,2816]{1,0:T(8,128)(2,1)} %all-gather.12.cloned.1.call-done) | copy-start | bytes 34603012
  417.3 11.9 %copy-start.13 = (bf16[1024,2048]{1,0:T(8,128)(2,1)S(1)}, bf16[1024,2048]{1,0:T(8,128)(2,1)}, u32[]{:S(2)}) copy-start(bf16[1024,2048]{1,0:T(8,128)(2,1)} %all-gather.10.cloned.1.call-done) | copy-start | bytes 12582916
Sparse Core Ops, SparseCore 0:
  12.3 19.9 all-gather.5
  34.0 138.9 all-gather.7
  244.7 17.4 all-gather.9
  263.7 153.5 all-gather.11
  418.8 158.2 all-gather.13
where the time goes:
time: 639 us; the launch traced here: 638 us
  waiting for transfers between devices  458 us (72%)
  matrix products  66.7 us (10%)
  blocking collectives  55.7 us (9%)
  other arithmetic  24.3 us (4%)
  between operations  13.5 us (2%)
  local copies, waits for them, and re-layouts  9.83 us (2%)
  starting transfers between devices  9.54 us (1%)
    all_gather x2, waiting for transfers between devices, in_one_piece(): out, at, done = (lax.all_gather(both, axis, axis=dim, tiled=True), 0, [])  296 us
    all_gather x1, waiting for transfers between devices, body(): down_full = lax.all_gather(w_down, 'fs', axis=1, tiled=True)  139 us
    all_to_all x2, blocking collectives, sent_and_summed(): lax.all_to_all(in_blocks(shard, dim, length), axis, 0, 0, tiled=True)  55.7 us
    dot_general x1, matrix products, body(): jnp.dot(activ, down_full, preferred_element_type=jnp.float32)  23 us
    all_gather x1, waiting for transfers between devices, body(): pieces = lax.all_gather(normed_ffn, 'tp', axis=0, tiled=True)  15.1 us
  transfers between devices with their start and end apart: 6, of which 5 were waited for; matrix products, arithmetic and copies ran while one was open for 9% of the time, Pallas kernels for 0%

commit v1 on v0

--- a/solution.py
+++ b/solution.py
@@ -187,7 +187,9 @@
     activ = (jax.nn.silu(causal_taps(gate_pre, gate_taps)) * causal_taps(up_pre, up_taps)).astype(
         jnp.bfloat16
     )
-    down_full = lax.all_gather(w_down, "fs", axis=1, tiled=True)
+    down_full = jnp.concatenate(
+        lax.all_to_all(jnp.stack([w_down] * lax.axis_size("fs")), "fs", 0, 0), axis=1
+    )
     ffn_sum = sent_and_summed(
         jnp.dot(activ, down_full, preferred_element_type=jnp.float32).astype(jnp.bfloat16), "tp", 0
     )

time: 639 us -> 544 us (0.85)
  waiting for transfers between devices: 458 us -> 356 us
  starting transfers between devices: 9.54 us -> 16.1 us
    all_gather x1 -> x0, waiting for transfers between devices: 139 us -> none  [body(): down_full = lax.all_gather(w_down, 'fs', axis=1, tiled=True)]
    all_gather x2, waiting for transfers between devices: 296 us -> 343 us  [in_one_piece(): out, at, done = (lax.all_gather(both, axis, axis=dim, tiled=True), 0, [])]
    all_gather x1, waiting for transfers between devices: 15.1 us -> 6.05 us  [body(): pieces = lax.all_gather(normed_ffn, 'tp', axis=0, tiled=True)]
    all_to_all x0 -> x1, starting transfers between devices: none -> 6.61 us  [body(): lax.all_to_all(jnp.stack([w_down] * lax.axis_size('fs')), 'fs', 0, 0)]
  transfers between devices with their start and end apart: 6 -> 6, of which waited for: 5 -> 4; matrix products, arithmetic and copies ran while one was open for 9% -> 12% of each run, Pallas kernels for 0% -> 0%
where the time goes in v1:
time: 544 us; the launch traced here: 542 us
  waiting for transfers between devices  356 us (65%)
  matrix products  67.1 us (12%)
  blocking collectives  51.8 us (10%)
  other arithmetic  25.1 us (5%)
  starting transfers between devices  16.1 us (3%)
  between operations  13.5 us (2%)
  local copies, waits for them, and re-layouts  12.2 us (2%)
    all_gather x2, waiting for transfers between devices, in_one_piece(): out, at, done = (lax.all_gather(both, axis, axis=dim, tiled=True), 0, [])  343 us
    all_to_all x2, blocking collectives, sent_and_summed(): lax.all_to_all(in_blocks(shard, dim, length), axis, 0, 0, tiled=True)  51.8 us
    dot_general x1, matrix products, body(): jnp.dot(activ, down_full, preferred_element_type=jnp.float32)  22.4 us
    dot_general x1, matrix products, body(): jnp.dot(pieces, gate_w, preferred_element_type=jnp.float32)  11.8 us
  transfers between devices with their start and end apart: 6, of which 4 were waited for; matrix products, arithmetic and copies ran while one was open for 12% of the time, Pallas kernels for 0%

profile of v1, /device:TPU:1, one launch (start us, length us, event | category | flops | bytes accessed | tf_op | source)
XLA Modules:
  0.0 542.2 jit_solution(1547383030648804760)
XLA Ops:
  6.6 2.1 fusion.6
  8.7 3.5 fusion.8
  12.3 0.7 pad_maximum_fusion.2
  13.0 1.5 broadcast_in_dim.25
  14.5 9.3 %all-to-all-start = ((bf16[32,512,64]{1,2,0:T(8,128)(2,1)}), bf16[32,512,64]{1,2,0:T(8,128)(2,1)}, u32[]{:S(2)}, u32[]{:S(2)}) async-start(bf16[32,512,64]{1,2,0:T(8,128)(2,1)} %broadcast_in_dim.25), calls=%async_computation | async-start | bytes 4194304 | tf_op jit(solution)/shard_map/all_to_all | solution.py:26
  24.2 1.0 fusion.44
  25.2 7.1 %all-gather.5.cloned.1.call-done = bf16[1024,2048]{1,0:T(8,128)(2,1)} async-done(((bf16[512,2048]{1,0:T(8,128)(2,1)}), bf16[1024,2048]{1,0:T(8,128)(2,1)}) %all-gather.5.cloned.1.call-update) | async-done | bytes 4194320 | tf_op jit(solution)/shard_map/all_gather | solution.py:147
  32.3 140.6 %all-gather.7.cloned.1.call-done = bf16[2048,1024]{1,0:T(8,128)(2,1)} async-done(((bf16[64,1024]{1,0:T(8,128)(2,1)}), bf16[2048,1024]{1,0:T(8,128)(2,1)}) %all-gather.7.cloned.1.call-update) | async-done | bytes 4194320 | tf_op jit(solution)/shard_map/all_gather | solution.py:17
  172.9 3.9 convolution_convert_fusion.3
  176.8 0.1 convert.17
  177.0 2.5 convolution_convert_fusion.2
  179.5 0.1 convert.18
  179.6 1.1 subtract_convert_fusion
  180.8 0.4 copy.41
  181.3 0.4 copy.42
  181.7 6.2 %fusion.31 = bf16[1024,512]{1,0:T(8,128)(2,1)} fusion(bf16[1024,2048]{1,0:T(8,128)(2,1)} %all-gather.5.cloned.1.call-done, bf16[2048,1024]{1,0:T(8,128)(2,1)} %all-gather.7.cloned.1.call-done), kind=kOutput, calls=%fused_computation.39 | convolution fusion | flops 2148007936 | bytes 7340032 | tf_op jit(solution)/shard_map/dot_general | solution.py:152
  187.8 1.3 reshape_reshape.3
  189.2 1.1 fusion.37
  190.3 1.6 fusion.38
  191.9 6.5 %while.13 = (s32[]{:T(128)}, f32[2,128,256]{2,1,0:T(8,128)S(1)}, bf16[8,2,128,256]{3,2,1,0:T(8,128)(2,1)}, f32[8,2,128,256]{3,2,1,0:T(8,128)S(1)}, s32[]{:T(128)}, /*index=5*/s32[]{:T(128)}, s32[]{:T(128)}) while((s32[]{:T(128)}, f32[2,128,256]{2,1,0:T(8,128)S(1)}, bf16[8,2,128,256]{3,2,1,0:T(8,128)(2,1)}, ...), condition=%wide.region_2.3_spmd.clone, body=%wide.region_1.2_spmd.clone.sunk | while | flops 262155 | bytes 1180272 | solution.py:99
  191.9 0.7 bitcast_dynamic-update-slice_fusion.2
  192.6 0.1 bitcast_add_fusion.2
  192.7 0.7 bitcast_dynamic-update-slice_fusion.2
  193.4 0.1 bitcast_add_fusion.2
  193.5 0.7 bitcast_dynamic-update-slice_fusion.2
  194.2 0.1 bitcast_add_fusion.2
  194.4 0.7 bitcast_dynamic-update-slice_fusion.2
  195.0 0.1 bitcast_add_fusion.2
  195.2 0.7 bitcast_dynamic-update-slice_fusion.2
  195.9 0.1 bitcast_add_fusion.2
  196.0 0.7 bitcast_dynamic-update-slice_fusion.2
  196.7 0.1 bitcast_add_fusion.2
  196.8 0.7 bitcast_dynamic-update-slice_fusion.2
  197.5 0.1 bitcast_add_fusion.2
  197.6 0.7 bitcast_dynamic-update-slice_fusion.2
  198.3 0.1 bitcast_add_fusion.2
  198.4 1.0 copy.49
  199.4 0.3 copy.39
  199.7 1.2 copy.50
  200.9 0.3 copy.40
  201.2 3.2 fusion.45
  204.5 3.0 fusion.54
  207.5 0.1 copy.46
  207.7 0.7 multiply_reduce_fusion
  208.3 0.9 fusion.29
  209.2 0.5 copy.47
  209.8 4.0 convolution_convert_fusion.1
  213.8 27.3 %all_to_all.20 = bf16[2,512,2048]{2,1,0:T(8,128)(2,1)S(1)} all-to-all(bf16[2,512,2048]{2,1,0:T(8,128)(2,1)S(1)} %bitcast.76), channel_id=1, replica_groups=mesh['rep'=2,'fs'=32,'tp'=2] {'tp'}, dimensions={0} | all-to-all | bytes 8388608 | tf_op jit(solution)/shard_map/all_to_all | solution.py:50
  241.1 1.0 convert_reduce_fusion.1
  242.1 0.6 copy-done
  242.7 0.7 fusion.10
  243.4 1.9 fusion.12
  245.4 0.8 pad_maximum_fusion.1
  246.2 3.2 stack.2
  249.4 6.6 %all-to-all-start.2 = ((bf16[32,1408,64]{1,2,0:T(8,128)(2,1)}), bf16[32,1408,64]{1,2,0:T(8,128)(2,1)}, u32[]{:S(2)}, u32[]{:S(2)}) async-start(bf16[32,1408,64]{1,2,0:T(8,128)(2,1)} %stack.2), calls=%async_computation.2 | async-start | bytes 11534336 | tf_op jit(solution)/shard_map/all_to_all | solution.py:191
  256.0 1.0 dynamic-slice_reduce_fusion.2
  257.0 6.0 %all-gather.9.cloned.1.call-done = bf16[1024,2048]{1,0:T(8,128)(2,1)} async-done(((bf16[512,2048]{1,0:T(8,128)(2,1)}), bf16[1024,2048]{1,0:T(8,128)(2,1)}) %all-gather.9.cloned.1.call-update) | async-done | bytes 4194320 | tf_op jit(solution)/shard_map/all_gather | solution.py:175
  263.1 202.3 %all-gather.11.cloned.1.call-done = bf16[2048,2816]{1,0:T(8,128)(2,1)} async-done(((bf16[64,2816]{1,0:T(8,128)(2,1)}), bf16[2048,2816]{1,0:T(8,128)(2,1)}) %all-gather.11.cloned.1.call-update) | async-done | bytes 11534352 | tf_op jit(solution)/shard_map/all_gather | solution.py:17
  465.4 11.8 %fusion.17 = f32[1024,1408]{1,0:T(8,128)} fusion(bf16[1024,2048]{1,0:T(8,128)(2,1)} %all-gather.9.cloned.1.call-done, bf16[2048,2816]{1,0:T(8,128)(2,1)} %all-gather.11.cloned.1.call-done), kind=kOutput, calls=%fused_computation.26 | convolution fusion | flops 5908463616 | bytes 15728640 | tf_op jit(solution)/shard_map/dot_general | solution.py:178
  477.2 8.5 %fusion.23 = f32[1024,1408]{1,0:T(8,128)} fusion(bf16[1024,2048]{1,0:T(8,128)(2,1)S(1)} %copy-done.13, bf16[2048,2816]{1,0:T(8,128)(2,1)S(1)} %copy-done.11), kind=kOutput, calls=%fused_computation.28 | convolution fusion | flops 5908463616 | bytes 15728640 | tf_op jit(solution)/shard_map/dot_general | solution.py:179
  485.7 22.4 %convolution_convert_fusion = bf16[1024,2048]{1,0:T(8,128)(2,1)} fusion(bf16[1408,2048]{0,1:T(8,128)(2,1)} %bitcast.14, f32[1024,1408]{1,0:T(8,128)} %fusion.23, f32[1024,1408]{1,0:T(8,128)} %fusion.17, f32[1408]{0:T(1024)S(1)} %get-tuple-element.59, f32[1408]{0:T(1024)S(1)} %get-tuple-element.58, f32[1408]{0:T(1024)S(1)} %get-tuple-element.57, ...), kind=kOutput, calls=%fused_computation.29 | convolution fusion | flops 5930745856 | bytes 21529600 | tf_op jit(solution)/shard_map/dot_general | solution.py:194
  508.1 24.5 %all_to_all.21 = bf16[2,512,2048]{2,1,0:T(8,128)(2,1)S(1)} all-to-all(bf16[2,512,2048]{2,1,0:T(8,128)(2,1)} %bitcast.75), channel_id=1, replica_groups=mesh['rep'=2,'fs'=32,'tp'=2] {'tp'}, dimensions={0} | all-to-all | bytes 8388608 | tf_op jit(solution)/shard_map/all_to_all | solution.py:50
  532.6 1.0 convert_reduce_fusion
  533.6 2.1 fusion.13
  (60 shorter events, 0.9 us)
Async XLA Ops:
  6.5 5.7 %copy-start.9 = (bf16[64,256]{1,0:T(8,128)(2,1)S(1)}, bf16[64,256]{1,0:T(8,128)(2,1)}, u32[]{:S(2)}) copy-start(bf16[64,256]{1,0:T(8,128)(2,1)} %param.16) | copy-start | bytes 98308
  6.5 5.7 %copy-start.8 = (bf16[64,256]{1,0:T(8,128)(2,1)S(1)}, bf16[64,256]{1,0:T(8,128)(2,1)}, u32[]{:S(2)}) copy-start(bf16[64,256]{1,0:T(8,128)(2,1)} %param.17) | copy-start | bytes 98308
  6.5 5.7 %copy-start.7 = (bf16[64,512]{1,0:T(8,128)(2,1)S(1)}, bf16[64,512]{1,0:T(8,128)(2,1)}, u32[]{:S(2)}) copy-start(bf16[64,512]{1,0:T(8,128)(2,1)} %param.18) | copy-start | bytes 196612
  6.5 6.4 %copy-start.6 = (bf16[512,64]{0,1:T(8,128)(2,1)S(1)}, bf16[512,64]{0,1:T(8,128)(2,1)}, u32[]{:S(2)}) copy-start(bf16[512,64]{0,1:T(8,128)(2,1)} %param.19) | copy-start | bytes 196612
  6.5 25.8 %all-gather.5.cloned.1.call-start = ((), (), s32[]{:S(2)}) async-start(), calls=%async_computation.4 | async-start | bytes 6291456 | tf_op jit(solution)/shard_map/all_gather | solution.py:147
  12.2 160.7 %all-gather.7.cloned.1.call-start = ((), (), s32[]{:S(2)}) async-start(), calls=%async_computation.5 | async-start | bytes 4325376 | tf_op jit(solution)/shard_map/all_gather | solution.py:17
  14.5 195.2 %all-to-all-start = ((bf16[32,512,64]{1,2,0:T(8,128)(2,1)}), bf16[32,512,64]{1,2,0:T(8,128)(2,1)}, u32[]{:S(2)}, u32[]{:S(2)}) async-start(bf16[32,512,64]{1,2,0:T(8,128)(2,1)} %broadcast_in_dim.25), calls=%async_computation | async-start | bytes 4194304 | tf_op jit(solution)/shard_map/all_to_all | solution.py:26
  23.9 239.2 %all-gather.9.cloned.1.call-start = ((), (), s32[]{:S(2)}) async-start(), calls=%async_computation.6 | async-start | bytes 6291456 | tf_op jit(solution)/shard_map/all_gather | solution.py:175
  172.9 4.1 copy-start.12
  199.7 4.8 copy-start.1
  201.2 3.2 copy-start.2
  241.1 1.6 copy-start
  242.7 0.7 copy-start.10
  243.4 2.0 copy-start.4
  243.4 2.0 copy-start.5
  243.4 2.8 copy-start.3
  245.3 220.1 %all-gather.11.cloned.1.call-start = ((), (), s32[]{:S(2)}) async-start(), calls=%async_computation.7 | async-start | bytes 11894784 | tf_op jit(solution)/shard_map/all_gather | solution.py:17
  249.4 236.3 %all-to-all-start.2 = ((bf16[32,1408,64]{1,2,0:T(8,128)(2,1)}), bf16[32,1408,64]{1,2,0:T(8,128)(2,1)}, u32[]{:S(2)}, u32[]{:S(2)}) async-start(bf16[32,1408,64]{1,2,0:T(8,128)(2,1)} %stack.2), calls=%async_computation.2 | async-start | bytes 11534336 | tf_op jit(solution)/shard_map/all_to_all | solution.py:191
  465.4 11.8 %copy-start.11 = (bf16[2048,2816]{1,0:T(8,128)(2,1)S(1)}, bf16[2048,2816]{1,0:T(8,128)(2,1)}, u32[]{:S(2)}) copy-start(bf16[2048,2816]{1,0:T(8,128)(2,1)} %all-gather.11.cloned.1.call-done) | copy-start | bytes 34603012
  465.4 11.8 %copy-start.13 = (bf16[1024,2048]{1,0:T(8,128)(2,1)S(1)}, bf16[1024,2048]{1,0:T(8,128)(2,1)}, u32[]{:S(2)}) copy-start(bf16[1024,2048]{1,0:T(8,128)(2,1)} %all-gather.9.cloned.1.call-done) | copy-start | bytes 12582916
Sparse Core Ops, SparseCore 0:
  12.3 19.9 all-gather.4
  34.0 138.8 all-gather.6
  245.4 17.5 all-gather.8
  264.6 200.8 all-gather.10
